TPU v7x, 512 devices: a whole 4x4x16 slice. The times are simulated.
512 devices in a mesh: sp: 128 (over z, x, core), tp: 4 (over y).
Axes of the slice: x: 4, y: 4, z: 16, core: 2. Of those that a mesh axis runs over, the one named last changes fastest.
Arguments:
- tokens: bfloat16 [16384, 2048], P(('sp', 'tp')), may hold values from -6 to 6
- norm_gain: float32 [2048], replicated, may hold values from 0.1 to 1.9
- w_query: bfloat16 [2048, 512], P(None, 'tp'), may hold values from -0.125 to 0.125
- w_key: bfloat16 [2048, 512], P(None, 'tp'), may hold values from -0.125 to 0.125
- w_value: bfloat16 [2048, 512], P(None, 'tp'), may hold values from -0.125 to 0.125
- score_offset: float32 [8], P('tp'), may hold values from -13 to -3, as said below
- w_out: bfloat16 [512, 2048], P('tp'), may hold values from -0.25 to 0.25
Outputs:
- mixed: bfloat16 [16384, 2048], P(('sp', 'tp'))
Inputs may be any that keep to these rules, and one draw needn't show every extreme that they name: `score_offset`: one offset a head.
All inputs are finite; a program needn't handle non-finite values.
Results may differ from a plain program's by a relative error of at most 0.01.
Values may be sent and summed in bfloat16 or wider, within the bound.
A program may use at most 64 MiB of HBM per device.

v0:
```python
import math
import jax
import jax.numpy as jnp
from jax import lax
from jax.sharding import Mesh
from jax.sharding import PartitionSpec as P

HEAD_DIM = 64
SP = ("sp_0", "sp_1", "sp_2")
SP_TP = ("sp_0", "sp_1", "sp_2", "tp")
RMS_EPS = 1e-06


def in_order(tiles, dim):
    tiles = jnp.moveaxis(tiles, 0, dim)
    dims = tiles.shape
    return tiles.reshape(*dims[:dim], dims[dim] * dims[dim + 1], *dims[dim + 2 :])


def sent_to_all(array, axis):
    copies = jnp.broadcast_to(array, (lax.axis_size(axis), *array.shape))
    return lax.all_to_all(copies, axis, split_axis=0, concat_axis=0, tiled=True)


def collect(array, axis, dim):
    return in_order(sent_to_all(array, axis), dim)


def gather_in_order(array, axes, sequence):
    tiles = array[None]
    for k in sequence:
        tiles = lax.all_gather(tiles, axes[k], axis=0, tiled=True)
    block = [lax.axis_size(axes[k]) for k in reversed(sequence)]
    tiles = tiles.reshape(*block, *array.shape)
    turned = sorted(range(len(sequence)), key=lambda place: sequence[len(sequence) - 1 - place])
    return tiles.transpose(*turned, *range(len(sequence), tiles.ndim)).reshape(-1, *array.shape)


def gather_axes(array, axes, sequence, dim):
    return in_order(gather_in_order(array, axes, sequence), dim)


def cut_along(array, dim, count):
    dims = array.shape
    tiles = array.reshape(*dims[:dim], count, dims[dim] // count, *dims[dim + 1 :])
    return jnp.moveaxis(tiles, dim, 0)


def sent_and_summed(array, axis, dim):
    tiles = cut_along(array, dim, lax.axis_size(axis))
    arrived = lax.all_to_all(tiles, axis, split_axis=0, concat_axis=0, tiled=True)
    return arrived.astype(jnp.float32).sum(axis=0)


def per_device(tokens, norm_gain, w_query, w_key, w_value, score_offset, w_out):
    groups = lax.axis_size("tp")
    tok_rows = tokens.shape[0] * groups
    head_width = w_query.shape[1]
    heads_dev = score_offset.shape[0]
    rows_f32 = collect(tokens, "tp", 0).astype(jnp.float32)
    inv_rms = lax.rsqrt(jnp.mean(rows_f32 * rows_f32, axis=1, keepdims=True) + RMS_EPS)
    normed = (rows_f32 * inv_rms * norm_gain).astype(jnp.bfloat16)
    projected = jnp.concatenate(
        [
            jnp.dot(normed, w_query, preferred_element_type=jnp.float32),
            jnp.dot(normed, w_key, preferred_element_type=jnp.float32),
            jnp.dot(normed, w_value, preferred_element_type=jnp.float32),
        ],
        axis=1,
    ).astype(jnp.bfloat16)
    queries = projected[:, :head_width].reshape(tok_rows, heads_dev, HEAD_DIM)
    key_vals = jnp.stack(
        [projected[:, head_width : 2 * head_width], projected[:, 2 * head_width :]]
    )
    own_index = lax.axis_index(SP)
    query_pos = own_index * tok_rows + jnp.arange(tok_rows, dtype=jnp.int32)
    offsets = score_offset[:, None, None]

    def absorb(running, key_block, key_start):
        totals, log_kept = running
        key_rows = key_block.shape[1]
        key_part = key_block[0].reshape(key_rows, heads_dev, HEAD_DIM)
        value_part = key_block[1].reshape(key_rows, heads_dev, HEAD_DIM)
        key_pos = key_start + jnp.arange(key_rows, dtype=jnp.int32)
        scores = (
            jnp.einsum("qhd,khd->hqk", queries, key_part, preferred_element_type=jnp.float32)
            * HEAD_DIM ** (-0.5)
            + offsets
        )
        earlier = ((key_pos[None, :] < query_pos[:, None]) & (key_pos[None, :] >= 0))[None]
        log_keep = jnp.where(earlier, jax.nn.log_sigmoid(-scores), 0.0)
        suffix = lax.cumsum(log_keep, axis=2, reverse=True) - log_keep + log_kept[:, :, None]
        weights = jnp.where(earlier, jnp.exp(jax.nn.log_sigmoid(scores) + suffix), 0.0).astype(
            jnp.bfloat16
        )
        totals = totals + jnp.einsum(
            "hqk,khd->hqd", weights, value_part, preferred_element_type=jnp.float32
        )
        return (totals, log_kept + jnp.sum(log_keep, axis=2))

    start_state = (
        jnp.zeros((heads_dev, tok_rows, HEAD_DIM), jnp.float32),
        jnp.zeros((heads_dev, tok_rows), jnp.float32),
    )
    all_keys = gather_axes(key_vals, SP, (1, 0, 2), 1)
    total_rows = all_keys.shape[1]
    span_rows = math.gcd(total_rows, 2048)
    span_count = total_rows // span_rows

    def sweep(turn_idx, carried):
        span_start = ((span_count - 1 - turn_idx) * span_rows).astype(jnp.int32)
        key_block = lax.dynamic_slice_in_dim(all_keys, span_start, span_rows, 1)
        return absorb(carried, key_block, span_start)

    finished = lax.fori_loop(0, span_count, sweep, start_state)
    mixed_rows = finished[0].transpose(1, 0, 2).reshape(tok_rows, head_width).astype(jnp.bfloat16)
    return sent_and_summed(
        jnp.dot(mixed_rows, w_out, preferred_element_type=jnp.float32).astype(jnp.bfloat16), "tp", 0
    ).astype(jnp.bfloat16)


def solution(mesh):
    finer = Mesh(mesh.devices.reshape(16, 4, 2, mesh.shape["tp"]), ("sp_0", "sp_1", "sp_2", "tp"))
    placed = (
        P(SP_TP, None),
        P(),
        P(None, "tp"),
        P(None, "tp"),
        P(None, "tp"),
        P("tp"),
        P("tp", None),
    )
    return jax.shard_map(
        per_device, mesh=finer, in_specs=placed, out_specs=P(SP_TP, None), check_vma=False
    )
```

profile of v0, /device:TPU:1, one launch (start us, length us, event | category | flops | bytes accessed | tf_op | source)
XLA Modules:
  0.0 320.8 jit_solution(11479637697951911001)
XLA Ops:
  7.7 11.7 %all_to_all.10 = bf16[4,32,2048]{2,1,0:T(8,128)(2,1)S(1)} all-to-all(bf16[4,32,2048]{2,1,0:T(8,128)(2,1)S(1)} %broadcast_in_dim.56), channel_id=1, replica_groups=mesh['sp_0'=16,'sp_1'=4,'sp_2'=2,'tp'=4] {'tp'}, dimensions={0} | all-to-all | bytes 1048576 | tf_op jit(solution)/shard_map/all_to_all | solution.py:22
  20.5 12.1 %all-gather = bf16[8,128,128]{2,1,0:T(8,128)(2,1)} all-gather(bf16[2,128,128]{2,1,0:T(8,128)(2,1)S(1)} %pad_maximum_fusion), channel_id=2, replica_groups=mesh['sp_0'=16,'sp_1'=4,'sp_2'=2,'tp'=4] {'sp_1'}, dimensions={0}, use_global_device_ids=true | all-gather | bytes 327680 | tf_op jit(solution)/shard_map/all_gather | solution.py:32
  32.7 75.2 %all-gather.4.cloned.1.call-done = bf16[64,2,128,128]{3,2,1,0:T(8,128)(2,1)} async-done(((bf16[4,2,128,128]{3,2,1,0:T(8,128)(2,1)}), bf16[64,2,128,128]{3,2,1,0:T(8,128)(2,1)}) %all-gather.4.cloned.1.call-update) | async-done | bytes 4194320 | tf_op jit(solution)/shard_map/all_gather | solution.py:32
  109.3 37.7 %all-gather.6.cloned.1.call-done = bf16[128,2,128,128]{3,2,1,0:T(8,128)(2,1)} async-done(((bf16[64,2,128,128]{3,2,1,0:T(8,128)(2,1)}), bf16[128,2,128,128]{3,2,1,0:T(8,128)(2,1)}) %all-gather.6.cloned.1.call-update) | async-done | bytes 8388624 | tf_op jit(solution)/shard_map/all_gather | solution.py:32
  147.0 10.3 %copy.27 = bf16[16,4,2,2,128,128]{5,4,3,2,1,0:T(8,128)(2,1)} copy(bf16[16,4,2,2,128,128]{5,4,3,1,0,2:T(8,128)(2,1)} %bitcast.75) | data formatting | bytes 16777216 | tf_op jit(solution)/shard_map/transpose | solution.py:36
  157.3 10.3 %copy.28 = bf16[2,128,128,128]{3,2,1,0:T(8,128)(2,1)} copy(bf16[2,128,128,128]{3,2,0,1:T(8,128)(2,1)} %bitcast.72) | data formatting | bytes 16777216 | tf_op jit(solution)/shard_map/transpose | solution.py:15
  167.7 133.3 %while.16 = (s32[]{:T(128)}, f32[2,128,64]{1,2,0:T(8,128)S(1)}, f32[2,128]{1,0:T(2,128)S(1)}, bf16[2,16384,128]{2,1,0:T(8,128)(2,1)}, bf16[128,2,64]{0,2,1:T(8,1...) while((s32[]{:T(128)}, f32[2,128,64]{1,2,0:T(8,128)S(1)}, ...), condition=%wide.region_5.6_spmd.clone, body=%wide.region_1.5_spmd.clone.sunk | while | flops 218732672 | bytes 37794140 | solution.py:115
  170.9 3.2 fusion.46
  174.1 5.0 %fusion.47 = f32[2,128,16,128]{1,2,3,0:T(8,128)S(1)} fusion(f32[2,128,16,128]{1,3,2,0:T(8,128)S(1)} %bitcast.70), kind=kOutput, calls=%fused_computation.15.clone.1 | output fusion | flops 66584576 | bytes 4194304 | tf_op jit(solution)/shard_map/reduce-window.4
  187.6 3.2 fusion.46
  190.8 5.0 %fusion.47 = f32[2,128,16,128]{1,2,3,0:T(8,128)S(1)} fusion(f32[2,128,16,128]{1,3,2,0:T(8,128)S(1)} %bitcast.70), kind=kOutput, calls=%fused_computation.15.clone.1 | output fusion | flops 66584576 | bytes 4194304 | tf_op jit(solution)/shard_map/reduce-window.4
  204.2 3.2 fusion.46
  207.4 5.0 %fusion.47 = f32[2,128,16,128]{1,2,3,0:T(8,128)S(1)} fusion(f32[2,128,16,128]{1,3,2,0:T(8,128)S(1)} %bitcast.70), kind=kOutput, calls=%fused_computation.15.clone.1 | output fusion | flops 66584576 | bytes 4194304 | tf_op jit(solution)/shard_map/reduce-window.4
  220.9 3.2 fusion.46
  224.1 5.0 %fusion.47 = f32[2,128,16,128]{1,2,3,0:T(8,128)S(1)} fusion(f32[2,128,16,128]{1,3,2,0:T(8,128)S(1)} %bitcast.70), kind=kOutput, calls=%fused_computation.15.clone.1 | output fusion | flops 66584576 | bytes 4194304 | tf_op jit(solution)/shard_map/reduce-window.4
  237.6 3.2 fusion.46
  240.8 5.0 %fusion.47 = f32[2,128,16,128]{1,2,3,0:T(8,128)S(1)} fusion(f32[2,128,16,128]{1,3,2,0:T(8,128)S(1)} %bitcast.70), kind=kOutput, calls=%fused_computation.15.clone.1 | output fusion | flops 66584576 | bytes 4194304 | tf_op jit(solution)/shard_map/reduce-window.4
  254.3 3.2 fusion.46
  257.4 5.0 %fusion.47 = f32[2,128,16,128]{1,2,3,0:T(8,128)S(1)} fusion(f32[2,128,16,128]{1,3,2,0:T(8,128)S(1)} %bitcast.70), kind=kOutput, calls=%fused_computation.15.clone.1 | output fusion | flops 66584576 | bytes 4194304 | tf_op jit(solution)/shard_map/reduce-window.4
  270.9 3.2 fusion.46
  274.1 5.0 %fusion.47 = f32[2,128,16,128]{1,2,3,0:T(8,128)S(1)} fusion(f32[2,128,16,128]{1,3,2,0:T(8,128)S(1)} %bitcast.70), kind=kOutput, calls=%fused_computation.15.clone.1 | output fusion | flops 66584576 | bytes 4194304 | tf_op jit(solution)/shard_map/reduce-window.4
  287.6 3.2 fusion.46
  290.8 5.0 %fusion.47 = f32[2,128,16,128]{1,2,3,0:T(8,128)S(1)} fusion(f32[2,128,16,128]{1,3,2,0:T(8,128)S(1)} %bitcast.70), kind=kOutput, calls=%fused_computation.15.clone.1 | output fusion | flops 66584576 | bytes 4194304 | tf_op jit(solution)/shard_map/reduce-window.4
  301.4 11.9 %all_to_all.11 = bf16[4,32,2048]{2,1,0:T(8,128)(2,1)S(1)} all-to-all(bf16[4,32,2048]{2,1,0:T(8,128)(2,1)S(1)} %bitcast.76), channel_id=1, replica_groups=mesh['sp_0'=16,'sp_1'=4,'sp_2'=2,'tp'=4] {'tp'}, dimensions={0} | all-to-all | bytes 1048576 | tf_op jit(solution)/shard_map/all_to_all | solution.py:51
  (182 shorter events, 71.2 us)
Async XLA Ops:
  6.5 294.5 %copy-start = (bf16[128,2048]{1,0:T(8,128)(2,1)S(1)}, bf16[128,2048]{1,0:T(8,128)(2,1)}, u32[]{:S(2)}) copy-start(bf16[128,2048]{1,0:T(8,128)(2,1)} %param.15) | copy-start | bytes 1572868
  6.5 13.1 %copy-start.5 = (f32[2048]{0:T(1024)S(1)}, f32[2048]{0:T(1024)}, u32[]{:S(2)}) copy-start(f32[2048]{0:T(1024)} %param.10) | copy-start | bytes 24580
  6.5 13.3 %copy-start.2 = (bf16[2048,128]{1,0:T(8,128)(2,1)S(1)}, bf16[2048,128]{1,0:T(8,128)(2,1)}, u32[]{:S(2)}) copy-start(bf16[2048,128]{1,0:T(8,128)(2,1)} %param.13) | copy-start | bytes 1572868
  6.5 13.6 %copy-start.3 = (bf16[2048,128]{1,0:T(8,128)(2,1)S(1)}, bf16[2048,128]{1,0:T(8,128)(2,1)}, u32[]{:S(2)}) copy-start(bf16[2048,128]{1,0:T(8,128)(2,1)} %param.12) | copy-start | bytes 1572868
  6.5 101.4 %all-gather.4.cloned.1.call-start = ((), (), s32[]{:S(2)}) async-start(), calls=%async_computation.2 | async-start | bytes 4456448 | tf_op jit(solution)/shard_map/all_gather | solution.py:32
  32.7 114.3 %all-gather.6.cloned.1.call-start = ((), (), s32[]{:S(2)}) async-start(), calls=%async_computation.3 | async-start | bytes 12582912 | tf_op jit(solution)/shard_map/all_gather | solution.py:32
  107.9 1.0 copy-start.4
  157.3 10.4 %copy-start.6 = (f32[2]{0:T(128)S(1)}, f32[2]{0:T(128)}, u32[]{:S(2)}) copy-start(f32[2]{0:T(128)} %param.14) | copy-start | bytes 28
  179.4 1.6 copy-start.1
  181.0 3.3 %copy-start.7 = (f32[2]{0:T(128)S(1)}, f32[2]{0:T(128)}, u32[]{:S(2)}) copy-start(f32[2]{0:T(128)} %get-tuple-element.313) | copy-start | bytes 28 | tf_op jit(solution)/shard_map/while
  196.0 1.6 copy-start.1
  197.6 3.3 %copy-start.7 = (f32[2]{0:T(128)S(1)}, f32[2]{0:T(128)}, u32[]{:S(2)}) copy-start(f32[2]{0:T(128)} %get-tuple-element.313) | copy-start | bytes 28 | tf_op jit(solution)/shard_map/while
  212.7 1.6 copy-start.1
  214.3 3.3 %copy-start.7 = (f32[2]{0:T(128)S(1)}, f32[2]{0:T(128)}, u32[]{:S(2)}) copy-start(f32[2]{0:T(128)} %get-tuple-element.313) | copy-start | bytes 28 | tf_op jit(solution)/shard_map/while
  229.4 1.6 copy-start.1
  231.0 3.3 %copy-start.7 = (f32[2]{0:T(128)S(1)}, f32[2]{0:T(128)}, u32[]{:S(2)}) copy-start(f32[2]{0:T(128)} %get-tuple-element.313) | copy-start | bytes 28 | tf_op jit(solution)/shard_map/while
  246.1 1.6 copy-start.1
  247.7 3.3 %copy-start.7 = (f32[2]{0:T(128)S(1)}, f32[2]{0:T(128)}, u32[]{:S(2)}) copy-start(f32[2]{0:T(128)} %get-tuple-element.313) | copy-start | bytes 28 | tf_op jit(solution)/shard_map/while
  262.7 1.6 copy-start.1
  264.3 3.3 %copy-start.7 = (f32[2]{0:T(128)S(1)}, f32[2]{0:T(128)}, u32[]{:S(2)}) copy-start(f32[2]{0:T(128)} %get-tuple-element.313) | copy-start | bytes 28 | tf_op jit(solution)/shard_map/while
  279.4 1.6 copy-start.1
  281.0 3.3 %copy-start.7 = (f32[2]{0:T(128)S(1)}, f32[2]{0:T(128)}, u32[]{:S(2)}) copy-start(f32[2]{0:T(128)} %get-tuple-element.313) | copy-start | bytes 28 | tf_op jit(solution)/shard_map/while
  296.1 1.6 copy-start.1
  297.7 3.3 %copy-start.7 = (f32[2]{0:T(128)S(1)}, f32[2]{0:T(128)}, u32[]{:S(2)}) copy-start(f32[2]{0:T(128)} %get-tuple-element.313) | copy-start | bytes 28 | tf_op jit(solution)/shard_map/while
Sparse Core Ops, SparseCore 0:
  32.8 75.0 all-gather.3
  110.0 36.9 all-gather.5
where the time goes:
time: 322 us; the launch traced here: 321 us
  waiting for transfers between devices  113 us (35%)
  other arithmetic  79 us (25%)
  local copies, waits for them, and re-layouts  49.2 us (15%)
  blocking collectives  35.7 us (11%)
  matrix products  29.4 us (9%)
  between operations  13.5 us (4%)
    all_gather x2, waiting for transfers between devices, gather_in_order(): tiles = lax.all_gather(tiles, axes[k], axis=0, tiled=True)  113 us
    another operation x16, other arithmetic  40.8 us
    dot_general x8, matrix products, absorb(): jnp.einsum('qhd,khd->hqk', queries, key_part, preferred_element_type=jnp....  25.5 us
    convert_element_type x8, other arithmetic, absorb(): jnp.where(earlier, jnp.exp(jax.nn.log_sigmoid(scores) + suffix), 0.0)  23.9 us
    all_gather x1, blocking collectives, gather_in_order(): tiles = lax.all_gather(tiles, axes[k], axis=0, tiled=True)  12.1 us
    all_to_all x1, blocking collectives, sent_and_summed(): lax.all_to_all(tiles, axis, split_axis=0, concat_axis=0, tiled=True)  11.9 us
    and x8, other arithmetic, absorb(): (key_pos[None, :] < query_pos[:, None]) & (key_pos[None, :] >= 0)  11.8 us
    all_to_all x1, blocking collectives, sent_to_all(): return lax.all_to_all(copies, axis, split_axis=0, concat_axis=0, tiled=True)  11.7 us
  transfers between devices with their start and end apart: 2, of which 2 were waited for; matrix products, arithmetic and copies ran while one was open for 0% of the time, Pallas kernels for 0%

commit v1 on v0

--- a/solution.py
+++ b/solution.py
@@ -29,7 +29,10 @@
 def gather_in_order(array, axes, sequence):
     tiles = array[None]
     for k in sequence:
-        tiles = lax.all_gather(tiles, axes[k], axis=0, tiled=True)
+        point = axes[k]
+        tiles = jnp.concatenate(
+            lax.all_to_all(jnp.stack([tiles] * lax.axis_size(point), axis=0), point, 0, 0), axis=0
+        )
     block = [lax.axis_size(axes[k]) for k in reversed(sequence)]
     tiles = tiles.reshape(*block, *array.shape)
     turned = sorted(range(len(sequence)), key=lambda place: sequence[len(sequence) - 1 - place])

time: 322 us -> 420 us (1.30)
  waiting for transfers between devices: 113 us -> 181 us
  blocking collectives: 35.7 us -> 53.9 us
  starting transfers between devices: 0.08 us -> 15.1 us
  between operations: 13.5 us -> 0.16 us
  other arithmetic: 79 us -> 86.4 us
    all_to_all x0 -> x1, waiting for transfers between devices: none -> 181 us  [gather_in_order(): lax.all_to_all(jnp.stack([tiles] * lax.axis_size(point), axis=0), point,...]
    all_gather x2 -> x0, waiting for transfers between devices: 113 us -> none  [gather_in_order(): tiles = lax.all_gather(tiles, axes[k], axis=0, tiled=True)]
    all_to_all x0 -> x2, blocking collectives: none -> 30.6 us  [gather_in_order(): lax.all_to_all(jnp.stack([tiles] * lax.axis_size(point), axis=0), point,...]
    all_to_all x0 -> x1, starting transfers between devices: none -> 15.1 us  [gather_in_order(): lax.all_to_all(jnp.stack([tiles] * lax.axis_size(point), axis=0), point,...]
    another operation x16 -> x19, local copies, waits for them, and re-layouts: 0.08 us -> 13.4 us  [the longest x1 10.3 us: gather_in_order(): tiles = tiles.reshape(*block, *array.shape)]
    all_gather x1 -> x0, blocking collectives: 12.1 us -> none  [gather_in_order(): tiles = lax.all_gather(tiles, axes[k], axis=0, tiled=True)]
    transpose x1 -> x0, local copies, waits for them, and re-layouts: 10.3 us -> none  [gather_in_order(): tiles.transpose(*turned, *range(len(sequence), tiles.ndim))]
    another operation x16 -> x17, other arithmetic: 40.8 us -> 48.2 us
  transfers between devices with their start and end apart: 2 -> 1, of which waited for: 2 -> 1; matrix products, arithmetic and copies ran while one was open for 0% -> 0% of each run, Pallas kernels for 0% -> 0%
where the time goes in v1:
time: 420 us; the launch traced here: 419 us
  waiting for transfers between devices  181 us (43%)
  other arithmetic  86.4 us (21%)
  blocking collectives  53.9 us (13%)
  local copies, waits for them, and re-layouts  51.2 us (12%)
  matrix products  29.7 us (7%)
  starting transfers between devices  15.1 us (4%)
    all_to_all x1, waiting for transfers between devices, gather_in_order(): lax.all_to_all(jnp.stack([tiles] * lax.axis_size(point), axis=0), point,...  181 us
    another operation x16, other arithmetic  40.8 us
    all_to_all x2, blocking collectives, gather_in_order(): lax.all_to_all(jnp.stack([tiles] * lax.axis_size(point), axis=0), point,...  30.6 us
    dot_general x8, matrix products, absorb(): jnp.einsum('qhd,khd->hqk', queries, key_part, preferred_element_type=jnp....  25.8 us
    convert_element_type x8, other arithmetic, absorb(): jnp.where(earlier, jnp.exp(jax.nn.log_sigmoid(scores) + suffix), 0.0)  23.9 us
    all_to_all x1, starting transfers between devices, gather_in_order(): lax.all_to_all(jnp.stack([tiles] * lax.axis_size(point), axis=0), point,...  15.1 us
    and x8, other arithmetic, absorb(): (key_pos[None, :] < query_pos[:, None]) & (key_pos[None, :] >= 0)  11.8 us
    all_to_all x1, blocking collectives, sent_to_all(): return lax.all_to_all(copies, axis, split_axis=0, concat_axis=0, tiled=True)  11.7 us
  transfers between devices with their start and end apart: 1, of which 1 were waited for; matrix products, arithmetic and copies ran while one was open for 0% of the time, Pallas kernels for 0%

profile of v1, /device:TPU:1, one launch (start us, length us, event | category | flops | bytes accessed | tf_op | source)
XLA Modules:
  0.0 419.0 jit_solution(4414463520227936977)
XLA Ops:
  1.1 11.7 %all_to_all.25 = bf16[4,32,2048]{2,1,0:T(8,128)(2,1)S(1)} all-to-all(bf16[4,32,2048]{2,1,0:T(8,128)(2,1)S(1)} %broadcast_in_dim.53), channel_id=1, replica_groups=mesh['sp_0'=16,'sp_1'=4,'sp_2'=2,'tp'=4] {'tp'}, dimensions={0} | all-to-all | bytes 1048576 | tf_op jit(solution)/shard_map/all_to_all | solution.py:22
  14.0 11.0 %all_to_all.26 = bf16[4,1,2,128,128]{4,3,2,1,0:T(8,128)(2,1)S(1)} all-to-all(bf16[4,1,2,128,128]{4,3,2,1,0:T(8,128)(2,1)S(1)} %stack.21), channel_id=1, replica_groups=mesh['sp_0'=16,'sp_1'=4,'sp_2'=2,'tp'=4] {'sp_1'}, dimensions={0} | all-to-all | bytes 524288 | tf_op jit(solution)/shard_map/all_to_all | solution.py:34
  28.0 15.1 %all-to-all-start.2 = ((bf16[16,4,2,128,128]{4,3,2,1,0:T(8,128)(2,1)}), bf16[16,4,2,128,128]{4,3,2,1,0:T(8,128)(2,1)}, u32[]{:S(2)}, u32[]{:S(2)}) async-start(bf16[16,4,2,128,128]{4,3,2,1,0:T(8,128)(2,1)} %stack.22), calls=%async_computation.2 | async-start | bytes 8388608 | tf_op jit(solution)/shard_map/all_to_all | solution.py:34
  43.5 181.4 %all-to-all-done.2 = bf16[16,4,2,128,128]{4,3,2,1,0:T(8,128)(2,1)} async-done(((bf16[16,4,2,128,128]{4,3,2,1,0:T(8,128)(2,1)}), bf16[16,4,2,128,128]{4,3,2,1,0:T(8,128)(2,1)}, u32[]{:S(2)}, u32[]{:S(2)}) %all-to-all-start.2) | async-done | bytes 4194336 | tf_op jit(solution)/shard_map/all_to_all | solution.py:34
  224.9 7.5 %pad_maximum_fusion = bf16[2,64,2,128,128]{4,3,2,1,0:T(8,128)(2,1)} fusion(bf16[1,64,2,128,128]{4,3,2,1,0:T(8,128)(2,1)} %bitcast.4), kind=kLoop, calls=%fused_computation.28 | loop fusion | flops 4194304 | bytes 12582912 | tf_op jit(solution)/shard_map/stack | solution.py:34
  232.4 19.5 %all_to_all.27 = bf16[2,64,2,128,128]{4,3,2,1,0:T(8,128)(2,1)} all-to-all(bf16[2,64,2,128,128]{4,3,2,1,0:T(8,128)(2,1)} %pad_maximum_fusion), channel_id=1, replica_groups=mesh['sp_0'=16,'sp_1'=4,'sp_2'=2,'tp'=4] {'sp_2'}, dimensions={0} | all-to-all | bytes 16777216 | tf_op jit(solution)/shard_map/all_to_all | solution.py:34
  251.9 10.3 %copy.34 = bf16[2,16,4,2,128,128]{5,4,3,0,2,1:T(8,128)(2,1)} copy(bf16[2,16,4,2,128,128]{5,4,3,2,1,0:T(8,128)(2,1)} %bitcast.73) | data formatting | bytes 16777216 | tf_op jit(solution)/shard_map/reshape;reshape | solution.py:37
  262.3 10.4 %copy.35 = bf16[2,128,128,128]{3,2,1,0:T(8,128)(2,1)} copy(bf16[2,128,128,128]{3,2,0,1:T(8,128)(2,1)} %bitcast.74) | data formatting | bytes 16777216 | tf_op jit(solution)/shard_map/transpose | solution.py:15
  272.6 133.6 %while.16 = (s32[]{:T(128)}, f32[2,128,64]{1,2,0:T(8,128)S(1)}, f32[2,128]{1,0:T(2,128)S(1)}, bf16[2,16384,128]{2,1,0:T(8,128)(2,1)}, bf16[128,2,64]{0,2,1:T(8,1...) while((s32[]{:T(128)}, f32[2,128,64]{1,2,0:T(8,128)S(1)}, ...), condition=%wide.region_5.6_spmd.clone, body=%wide.region_1.5_spmd.clone.sunk | while | flops 218732672 | bytes 37794140 | solution.py:118
  275.8 3.2 fusion.46
  279.1 5.0 %fusion.47 = f32[2,128,16,128]{1,2,3,0:T(8,128)S(1)} fusion(f32[2,128,16,128]{1,3,2,0:T(8,128)S(1)} %bitcast.71), kind=kOutput, calls=%fused_computation.15.clone.1 | output fusion | flops 66584576 | bytes 4194304 | tf_op jit(solution)/shard_map/reduce-window.4
  292.6 3.2 fusion.46
  295.8 5.0 %fusion.47 = f32[2,128,16,128]{1,2,3,0:T(8,128)S(1)} fusion(f32[2,128,16,128]{1,3,2,0:T(8,128)S(1)} %bitcast.71), kind=kOutput, calls=%fused_computation.15.clone.1 | output fusion | flops 66584576 | bytes 4194304 | tf_op jit(solution)/shard_map/reduce-window.4
  309.3 3.2 fusion.46
  312.5 5.0 %fusion.47 = f32[2,128,16,128]{1,2,3,0:T(8,128)S(1)} fusion(f32[2,128,16,128]{1,3,2,0:T(8,128)S(1)} %bitcast.71), kind=kOutput, calls=%fused_computation.15.clone.1 | output fusion | flops 66584576 | bytes 4194304 | tf_op jit(solution)/shard_map/reduce-window.4
  326.0 3.2 fusion.46
  329.2 5.0 %fusion.47 = f32[2,128,16,128]{1,2,3,0:T(8,128)S(1)} fusion(f32[2,128,16,128]{1,3,2,0:T(8,128)S(1)} %bitcast.71), kind=kOutput, calls=%fused_computation.15.clone.1 | output fusion | flops 66584576 | bytes 4194304 | tf_op jit(solution)/shard_map/reduce-window.4
  345.9 5.0 %fusion.47 = f32[2,128,16,128]{1,2,3,0:T(8,128)S(1)} fusion(f32[2,128,16,128]{1,3,2,0:T(8,128)S(1)} %bitcast.71), kind=kOutput, calls=%fused_computation.15.clone.1 | output fusion | flops 66584576 | bytes 4194304 | tf_op jit(solution)/shard_map/reduce-window.4
  359.4 3.2 fusion.46
  362.6 5.0 %fusion.47 = f32[2,128,16,128]{1,2,3,0:T(8,128)S(1)} fusion(f32[2,128,16,128]{1,3,2,0:T(8,128)S(1)} %bitcast.71), kind=kOutput, calls=%fused_computation.15.clone.1 | output fusion | flops 66584576 | bytes 4194304 | tf_op jit(solution)/shard_map/reduce-window.4
  379.3 5.0 %fusion.47 = f32[2,128,16,128]{1,2,3,0:T(8,128)S(1)} fusion(f32[2,128,16,128]{1,3,2,0:T(8,128)S(1)} %bitcast.71), kind=kOutput, calls=%fused_computation.15.clone.1 | output fusion | flops 66584576 | bytes 4194304 | tf_op jit(solution)/shard_map/reduce-window.4
  392.8 3.2 fusion.46
  396.0 5.0 %fusion.47 = f32[2,128,16,128]{1,2,3,0:T(8,128)S(1)} fusion(f32[2,128,16,128]{1,3,2,0:T(8,128)S(1)} %bitcast.71), kind=kOutput, calls=%fused_computation.15.clone.1 | output fusion | flops 66584576 | bytes 4194304 | tf_op jit(solution)/shard_map/reduce-window.4
  406.6 11.6 %all_to_all.28 = bf16[4,32,2048]{2,1,0:T(8,128)(2,1)S(1)} all-to-all(bf16[4,32,2048]{2,1,0:T(8,128)(2,1)S(1)} %bitcast.77), channel_id=1, replica_groups=mesh['sp_0'=16,'sp_1'=4,'sp_2'=2,'tp'=4] {'tp'}, dimensions={0} | all-to-all | bytes 1048576 | tf_op jit(solution)/shard_map/all_to_all | solution.py:54
  (182 shorter events, 79.5 us)
Async XLA Ops:
  0.0 406.3 %copy-start = (bf16[128,2048]{1,0:T(8,128)(2,1)S(1)}, bf16[128,2048]{1,0:T(8,128)(2,1)}, u32[]{:S(2)}) copy-start(bf16[128,2048]{1,0:T(8,128)(2,1)} %param.15) | copy-start | bytes 1572868
  0.0 13.1 %copy-start.5 = (f32[2048]{0:T(1024)S(1)}, f32[2048]{0:T(1024)}, u32[]{:S(2)}) copy-start(f32[2048]{0:T(1024)} %param.10) | copy-start | bytes 24580
  0.0 13.3 %copy-start.2 = (bf16[2048,128]{1,0:T(8,128)(2,1)S(1)}, bf16[2048,128]{1,0:T(8,128)(2,1)}, u32[]{:S(2)}) copy-start(bf16[2048,128]{1,0:T(8,128)(2,1)} %param.13) | copy-start | bytes 1572868
  0.0 13.6 %copy-start.3 = (bf16[2048,128]{1,0:T(8,128)(2,1)S(1)}, bf16[2048,128]{1,0:T(8,128)(2,1)}, u32[]{:S(2)}) copy-start(bf16[2048,128]{1,0:T(8,128)(2,1)} %param.12) | copy-start | bytes 1572868
  28.0 15.1 %copy-start.4 = (bf16[2048,128]{1,0:T(8,128)(2,1)S(1)}, bf16[2048,128]{1,0:T(8,128)(2,1)}, u32[]{:S(2)}) copy-start(bf16[2048,128]{1,0:T(8,128)(2,1)} %param.11) | copy-start | bytes 1572868
  28.0 196.9 %all-to-all-start.2 = ((bf16[16,4,2,128,128]{4,3,2,1,0:T(8,128)(2,1)}), bf16[16,4,2,128,128]{4,3,2,1,0:T(8,128)(2,1)}, u32[]{:S(2)}, u32[]{:S(2)}) async-start(bf16[16,4,2,128,128]{4,3,2,1,0:T(8,128)(2,1)} %stack.22), calls=%async_computation.2 | async-start | bytes 8388608 | tf_op jit(solution)/shard_map/all_to_all | solution.py:34
  262.3 10.4 %copy-start.6 = (f32[2]{0:T(128)S(1)}, f32[2]{0:T(128)}, u32[]{:S(2)}) copy-start(f32[2]{0:T(128)} %param.14) | copy-start | bytes 28
  284.4 1.6 copy-start.1
  285.9 3.3 copy-start.7
  301.1 1.6 copy-start.1
  302.7 3.3 copy-start.7
  317.8 1.6 copy-start.1
  319.4 3.3 copy-start.7
  334.5 1.6 copy-start.1
  336.1 3.3 copy-start.7
  351.2 1.6 copy-start.1
  352.8 3.3 copy-start.7
  367.9 1.6 copy-start.1
  369.5 3.3 copy-start.7
  384.6 1.6 copy-start.1
  386.2 3.3 copy-start.7
  401.3 1.6 copy-start.1
  402.9 3.3 copy-start.7
